TPU v7x, 32 devices: a whole 2x2x4 slice. The times are simulated.
32 devices in a mesh: ep: 4 (over y, x), tp: 8 (over z, core).
Axes of the slice: x: 2, y: 2, z: 4, core: 2. Of those that a mesh axis runs over, the one named last changes fastest.
Arguments:
- tokens: bfloat16 [64, 2048], P('ep', 'tp'), may hold values from -6 to 6
- key_cache: bfloat16 [64, 16, 1024, 128], P('ep', 'tp'), may hold values from -1700 to 1700
- value_cache: bfloat16 [64, 16, 1024, 128], P('ep', 'tp'), may hold values from -6 to 6
- gate_totals: float32 [64, 16, 1024], P('ep', 'tp'), as said below
- lengths: int32 [64], P('ep'), may hold values from 128 to 1024
- attn_gain: float32 [2048], replicated, may hold values from 0.1 to 1.9
- w_query: bfloat16 [2048, 2048], P(None, 'tp'), may hold values from -0.125 to 0.125
- w_key: bfloat16 [2048, 2048], P(None, 'tp'), may hold values from -0.125 to 0.125
- w_value: bfloat16 [2048, 2048], P(None, 'tp'), may hold values from -0.125 to 0.125
- w_forget: bfloat16 [2048, 16], replicated, may hold values from -0.125 to 0.125
- forget_bias: float32 [16], replicated, may hold values from -3 to 0
- w_attn_out: bfloat16 [2048, 2048], P('tp'), may hold values from -0.1875 to 0.1875
- moe_gain: float32 [2048], replicated, may hold values from 0.1 to 1.9
- group_ids: int32 [64, 1], P('ep'), may hold values from 0 to 3; in each aligned block of 16 rows (0 to 15, 16 to 31, ...) at most 8 rows name the same one
- inner_ids: int32 [64, 2], P('ep'), may hold values from 0 to 3, all different within a row
- group_prob: float32 [64], P('ep'), may hold values from 0.2 to 1
- pair_logits: float32 [64, 2], P('ep'), may hold values from -6 to 6
- w_expert_gate: bfloat16 [4, 2048, 2048], P('ep', None, 'tp'), may hold values from -0.125 to 0.125
- w_expert_up: bfloat16 [4, 2048, 2048], P('ep', None, 'tp'), may hold values from -0.125 to 0.125
- w_expert_down: bfloat16 [4, 2048, 2048], P('ep', 'tp'), may hold values from -0.375 to 0.375
- w_dense_in: bfloat16 [2048, 2048], P(None, 'tp'), may hold values from -0.125 to 0.125
- w_dense_out: bfloat16 [2048, 2048], P('tp'), may hold values from -0.1875 to 0.1875
- dense_gate: float32 [2048], P('tp'), may hold values from -2 to 2
Outputs:
- layer_output: bfloat16 [64, 2048], P('ep', 'tp')
- new_keys: bfloat16 [64, 16, 128], P('ep', 'tp')
- new_values: bfloat16 [64, 16, 128], P('ep', 'tp')
- new_gates: float32 [64, 16], P('ep', 'tp')
Inputs may be any that keep to these rules, and one draw needn't show every extreme that they name: `group_ids`: within the 16 sequences of each index of ep (aligned blocks of rows), no group is named by more than 8 sequences, a bound that some block reaches. `inner_ids`: each row names 2 different experts of its group. `gate_totals`: along positions the values of each sequence and head never rise.
All inputs are finite; a program needn't handle non-finite values.
Results may differ from a plain program's by a relative error of at most 0.011.
Values may be sent and summed in bfloat16 or wider, within the bound.
A program may use at most 64 MiB of HBM per device.

v0:
```python
import jax
import jax.numpy as jnp
from jax import lax
from jax.sharding import PartitionSpec as P

FFE = 512
EPG = 4
EPS = 1e-06
FLOOR = -1e30


def norm_rows(row_data, gain_vec):
    values = row_data.astype(jnp.float32)
    factor = lax.rsqrt(jnp.mean(values * values, axis=-1, keepdims=True) + EPS)
    return (values * factor * gain_vec).astype(jnp.bfloat16)


def head_norm(values):
    factor = lax.rsqrt(jnp.mean(values * values, axis=-1, keepdims=True) + EPS)
    return (values * factor).astype(jnp.bfloat16)


def attend(queries, fresh_key, fresh_value, key_cache, value_cache, gate_totals, lengths, current):
    score_scale = queries.shape[-1] ** (-0.5)
    scores = (
        jnp.einsum("shd,shld->shl", queries, key_cache, preferred_element_type=jnp.float32)
        * score_scale
    )
    scores = scores + current[:, :, None] - gate_totals
    entry_indices = jnp.arange(key_cache.shape[2])
    live_mask = (entry_indices[None, :] < lengths[:, None])[:, None, :]
    scores = jnp.where(live_mask, scores, FLOOR)
    own_score = (
        jnp.sum(queries.astype(jnp.float32) * fresh_key.astype(jnp.float32), axis=-1) * score_scale
    )
    peak = jnp.maximum(jnp.max(scores, axis=-1), own_score)
    expo_terms = jnp.where(live_mask, jnp.exp(scores - peak[:, :, None]), 0.0)
    own_expo = jnp.exp(own_score - peak)
    denom_sum = jnp.sum(expo_terms, axis=-1) + own_expo
    weights = (expo_terms / denom_sum[:, :, None]).astype(jnp.bfloat16)
    own_weight = (own_expo / denom_sum).astype(jnp.bfloat16)
    attended = jnp.einsum("shl,shld->shd", weights, value_cache, preferred_element_type=jnp.float32)
    attended = attended + own_weight.astype(jnp.float32)[:, :, None] * fresh_value.astype(
        jnp.float32
    )
    return attended.astype(jnp.bfloat16)


def body(
    tokens,
    key_cache,
    value_cache,
    gate_totals,
    lengths,
    attn_gain,
    w_query,
    w_key,
    w_value,
    w_forget,
    forget_bias,
    w_attn_out,
    moe_gain,
    group_ids,
    inner_ids,
    group_prob,
    pair_logits,
    w_expert_gate,
    w_expert_up,
    w_expert_down,
    w_dense_in,
    w_dense_out,
    dense_gate,
):
    gathered = lax.all_gather(tokens, "tp", axis=1, tiled=True)
    normed = norm_rows(gathered, attn_gain)
    seq_count = gathered.shape[0]
    heads_dev = key_cache.shape[1]
    head_dim = key_cache.shape[3]

    def project(weight):
        return jnp.dot(normed, weight, preferred_element_type=jnp.float32).reshape(
            seq_count, heads_dev, head_dim
        )

    queries = head_norm(project(w_query))
    new_keys = head_norm(project(w_key))
    new_values = project(w_value).astype(jnp.bfloat16)
    first_head = lax.axis_index("tp") * heads_dev
    forget_cols = lax.dynamic_slice_in_dim(w_forget, first_head, heads_dev, 1)
    forget_shift = lax.dynamic_slice_in_dim(forget_bias, first_head, heads_dev, 0)
    log_gate = jax.nn.log_sigmoid(
        jnp.dot(normed, forget_cols, preferred_element_type=jnp.float32) + forget_shift
    )
    entry_indices = jnp.arange(gate_totals.shape[2])
    at_last = (entry_indices[None, :] == (lengths - 1)[:, None])[:, None, :]
    new_gates = jnp.sum(jnp.where(at_last, gate_totals, 0.0), axis=2) + log_gate
    attended = attend(
        queries, new_keys, new_values, key_cache, value_cache, gate_totals, lengths, new_gates
    )
    partial_value = jnp.dot(
        attended.reshape(seq_count, heads_dev * head_dim),
        w_attn_out,
        preferred_element_type=jnp.float32,
    )
    piece_sum = lax.psum_scatter(partial_value, "tp", scatter_dimension=1, tiled=True)
    own_residual = (tokens.astype(jnp.float32) + piece_sum).astype(jnp.bfloat16)
    moe_in = norm_rows(lax.all_gather(own_residual, "tp", axis=1, tiled=True), moe_gain)
    groups = lax.axis_size("ep")
    capacity = max(2, 2 * seq_count // groups)
    first_share = jax.nn.sigmoid(pair_logits[:, 0] - pair_logits[:, 1])
    pair_share = group_prob[:, None] * jnp.stack([first_share, 1.0 - first_share], axis=1)
    inner_range = jnp.arange(EPG)
    spread = jnp.sum(
        jnp.where(inner_ids[:, :, None] == inner_range[None, None, :], pair_share[:, :, None], 0.0),
        axis=1,
    ).astype(jnp.bfloat16)
    choose = (group_ids == jnp.arange(groups)[None, :]).astype(jnp.int32)
    before = jnp.cumsum(choose, axis=0) - choose
    slot_of = group_ids[:, 0] * capacity + jnp.sum(before * choose, axis=1)
    slot_ids = jnp.arange(groups * capacity)
    send_map = (slot_of[None, :] == slot_ids[:, None]).astype(jnp.bfloat16)
    send_weights = jnp.dot(send_map, spread, preferred_element_type=jnp.float32).astype(
        jnp.bfloat16
    )
    send_rows = jnp.dot(send_map, moe_in, preferred_element_type=jnp.float32).astype(jnp.bfloat16)
    recv_rows, recv_weights = (
        lax.all_to_all(send_rows, "ep", split_axis=0, concat_axis=0, tiled=True),
        lax.all_to_all(send_weights, "ep", split_axis=0, concat_axis=0, tiled=True),
    )
    dense_hidden = jax.nn.silu(
        jnp.dot(moe_in, w_dense_in, preferred_element_type=jnp.float32)
    ).astype(jnp.bfloat16)
    dense_part = jnp.dot(dense_hidden, w_dense_out, preferred_element_type=jnp.float32)
    hidden_dev = w_expert_gate.shape[2]
    expert_index = lax.axis_index("tp") * hidden_dev // FFE
    route_col = jnp.sum(
        jnp.where(inner_range[None, :] == expert_index, recv_weights.astype(jnp.float32), 0.0),
        axis=1,
    )
    gate_pre = jnp.dot(recv_rows, w_expert_gate[0], preferred_element_type=jnp.float32)
    up_pre = jnp.dot(recv_rows, w_expert_up[0], preferred_element_type=jnp.float32)
    hidden = (jax.nn.silu(gate_pre) * up_pre * route_col[:, None]).astype(jnp.bfloat16)
    expert_part = jnp.dot(hidden, w_expert_down[0], preferred_element_type=jnp.float32)
    expert_sum, dense_sum = (
        lax.psum_scatter(expert_part, "tp", scatter_dimension=1, tiled=True),
        lax.psum_scatter(dense_part, "tp", scatter_dimension=1, tiled=True),
    )
    returned = lax.all_to_all(
        expert_sum.astype(jnp.bfloat16), "ep", split_axis=0, concat_axis=0, tiled=True
    )
    expert_out = lax.dot_general(
        send_map, returned, (((0,), (0,)), ((), ())), preferred_element_type=jnp.float32
    )
    layer_output = (
        own_residual.astype(jnp.float32) + expert_out + jax.nn.sigmoid(dense_gate) * dense_sum
    )
    return (layer_output.astype(jnp.bfloat16), new_keys, new_values, new_gates)


def solution(mesh):
    placed = (
        P("ep", "tp"),
        P("ep", "tp", None, None),
        P("ep", "tp", None, None),
        P("ep", "tp", None),
        P("ep"),
        P(),
        P(None, "tp"),
        P(None, "tp"),
        P(None, "tp"),
        P(),
        P(),
        P("tp", None),
        P(),
        P("ep", None),
        P("ep", None),
        P("ep"),
        P("ep", None),
        P("ep", None, "tp"),
        P("ep", None, "tp"),
        P("ep", "tp", None),
        P(None, "tp"),
        P("tp", None),
        P("tp"),
    )
    return jax.shard_map(
        body,
        mesh=mesh,
        in_specs=placed,
        out_specs=(P("ep", "tp"), P("ep", "tp", None), P("ep", "tp", None), P("ep", "tp")),
        check_vma=False,
    )
```

profile of v0, /device:TPU:0, one launch (start us, length us, event | category | flops | bytes accessed | tf_op | source)
XLA Modules:
  0.0 172.8 jit_solution(14352880859179264883)
XLA Ops:
  7.3 0.8 broadcast_add_fusion
  8.1 0.7 iota_compare_fusion.1
  8.8 15.9 %all_gather.6 = bf16[16,2048]{1,0:T(8,128)(2,1)S(1)} all-gather(bf16[16,256]{1,0:T(8,128)(2,1)} %param.23), channel_id=1, replica_groups=mesh['ep'=4,'tp'=8] {'tp'}, dimensions={1}, use_global_device_ids=true | all-gather | bytes 73728 | tf_op jit(solution)/shard_map/all_gather | solution.py:74
  24.8 1.5 fusion.67
  26.5 1.5 fusion.70
  28.2 1.1 select_reduce_fusion
  30.1 1.0 fusion.58
  31.9 5.6 %fusion.34 = f32[16,2,1,1024]{3,2,1,0:T(1,128)S(1)} fusion(bf16[16,2,1024,128]{3,2,1,0:T(8,128)(2,1)} %param.24, bf16[16,2,128,1]{2,1,0,3:T(2,128)(2,1)S(1)} %get-tuple-element.12), kind=kOutput, calls=%fused_computation.48 | convolution fusion | flops 8388608 | bytes 8527872 | tf_op jit(solution)/shard_map/shd,shld->shl/dot_general | solution.py:26
  38.9 4.7 %fusion.24 = f32[16,2,1,128]{3,2,1,0:T(1,128)S(1)} fusion(bf16[16,2,1024,128]{3,2,1,0:T(8,128)(2,1)} %param.25, bf16[16,2,1024,1]{2,1,0,3:T(2,128)(2,1)S(1)} %fusion.26), kind=kOutput, calls=%fused_computation.33 | convolution fusion | flops 8388608 | bytes 8470528 | tf_op jit(solution)/shard_map/shl,shld->shd/dot_general | solution.py:42
  43.7 2.1 %fusion.46 = f32[16,2048]{1,0:T(8,128)} fusion(bf16[256,2048]{1,0:T(8,128)(2,1)} %param.34, bf16[2,8,2,128]{3,2,1,0:T(2,128)(2,1)S(1)} %bitcast.56), kind=kOutput, calls=%fused_computation.66 | convolution fusion | flops 16777216 | bytes 1187840 | tf_op jit(solution)/shard_map/dot_general | solution.py:100
  47.0 3.7 %all-to-all-start.1 = ((bf16[4,8,4]{1,2,0:T(4,128)(2,1)}), bf16[4,8,4]{1,2,0:T(4,128)(2,1)S(1)}, u32[]{:S(2)}, u32[]{:S(2)}) async-start(bf16[4,8,4]{1,2,0:T(4,128)(2,1)} %copy.49), calls=%async_computation.2 | async-start | bytes 8192 | tf_op jit(solution)/shard_map/all_to_all | solution.py:128
  50.8 26.8 %reduce-scatter.4.cloned.1.call-done = f32[16,256]{1,0:T(8,128)} async-done(((f32[16,2048]{1,0:T(8,128)}), f32[16,256]{1,0:T(8,128)}) %reduce-scatter.4.cloned.1.call-update) | async-done | bytes 16400 | tf_op jit(solution)/shard_map/reduce_scatter | solution.py:105
  78.3 13.9 %all_gather.7 = bf16[16,2048]{1,0:T(8,128)(2,1)S(1)} all-gather(bf16[16,256]{1,0:T(8,128)(2,1)S(1)} %add_convert_fusion), channel_id=1, replica_groups=mesh['ep'=4,'tp'=8] {'tp'}, dimensions={1}, use_global_device_ids=true | all-gather | bytes 73728 | tf_op jit(solution)/shard_map/all_gather | solution.py:107
  92.4 0.9 fusion
  93.2 3.6 %all-to-all-start = ((bf16[4,8,2048]{2,1,0:T(8,128)(2,1)}), bf16[4,8,2048]{2,1,0:T(8,128)(2,1)S(1)}, u32[]{:S(2)}, u32[]{:S(2)}) async-start(bf16[4,8,2048]{2,1,0:T(8,128)(2,1)} %fusion), calls=%async_computation.1 | async-start | bytes 262144 | tf_op jit(solution)/shard_map/all_to_all | solution.py:127
  97.1 4.8 %all-to-all-done = bf16[4,8,2048]{2,1,0:T(8,128)(2,1)S(1)} async-done(((bf16[4,8,2048]{2,1,0:T(8,128)(2,1)}), bf16[4,8,2048]{2,1,0:T(8,128)(2,1)S(1)}, u32[]{:S(2)}, u32[]{:S(2)}) %all-to-all-start) | async-done | bytes 131104 | tf_op jit(solution)/shard_map/all_to_all | solution.py:127
  101.9 1.5 fusion.10
  103.4 2.7 %fusion.4 = f32[32,2048]{1,0:T(8,128)} fusion(bf16[1,256,2048]{2,1,0:T(8,128)(2,1)S(1)} %copy-done, bf16[1,2048,256]{2,1,0:T(8,128)(2,1)} %param.41, bf16[4,8,2048]{2,1,0:T(8,128)(2,1)S(1)} %all-to-all-done, f32[32,256]{1,0:T(8,128)S(1)} %fusion.10, f32[32]{0:T(128)S(1)} %mul.181), kind=kOutput, calls=%fused_computation.7 | convolution fusion | flops 67166208 | bytes 2523264 | tf_op jit(solution)/shard_map/dot_general | solution.py:143
  106.2 1.5 fusion.44
  107.7 26.1 %reduce-scatter.6.cloned.1.call-done = f32[32,256]{1,0:T(8,128)} async-done(((f32[32,2048]{1,0:T(8,128)}), f32[32,256]{1,0:T(8,128)}) %reduce-scatter.6.cloned.1.call-update) | async-done | bytes 32784 | tf_op jit(solution)/shard_map/reduce_scatter | solution.py:145
  133.7 1.4 convert_bitcast_fusion
  135.1 3.6 %all-to-all-start.2 = ((bf16[4,8,256]{2,1,0:T(8,128)(2,1)}), bf16[4,8,256]{2,1,0:T(8,128)(2,1)S(1)}, u32[]{:S(2)}, u32[]{:S(2)}) async-start(bf16[4,8,256]{2,1,0:T(8,128)(2,1)} %convert_bitcast_fusion), calls=%async_computation.4 | async-start | bytes 32768 | tf_op jit(solution)/shard_map/all_to_all | solution.py:148
  138.7 26.0 %reduce-scatter.8.cloned.1.call-done = f32[16,256]{1,0:T(8,128)} async-done(((f32[16,2048]{1,0:T(8,128)}), f32[16,256]{1,0:T(8,128)}) %reduce-scatter.8.cloned.1.call-update) | async-done | bytes 16400 | tf_op jit(solution)/shard_map/reduce_scatter | solution.py:146
  164.7 1.5 fusion.5
  (75 shorter events, 5.7 us)
Async XLA Ops:
  7.2 96.2 %copy-start = (bf16[1,256,2048]{2,1,0:T(8,128)(2,1)S(1)}, bf16[1,256,2048]{2,1,0:T(8,128)(2,1)}, u32[]{:S(2)}) copy-start(bf16[1,256,2048]{2,1,0:T(8,128)(2,1)} %param.42) | copy-start | bytes 3145732
  7.2 31.3 %copy-start.5 = (f32[2048]{0:T(1024)S(1)}, f32[2048]{0:T(1024)}, u32[]{:S(2)}) copy-start(f32[2048]{0:T(1024)} %param.28) | copy-start | bytes 24580
  7.2 30.3 %copy-start.4 = (f32[16,2,1024]{2,1,0:T(2,128)S(1)}, f32[16,2,1024]{2,1,0:T(2,128)}, u32[]{:S(2)}) copy-start(f32[16,2,1024]{2,1,0:T(2,128)} %param.26) | copy-start | bytes 393220
  7.2 31.3 %copy-start.3 = (bf16[2048,256]{1,0:T(8,128)(2,1)S(1)}, bf16[2048,256]{1,0:T(8,128)(2,1)}, u32[]{:S(2)}) copy-start(bf16[2048,256]{1,0:T(8,128)(2,1)} %param.31) | copy-start | bytes 3145732
  7.2 70.3 %reduce-scatter.4.cloned.1.call-start = ((), (), s32[]{:S(2)}) async-start(), calls=%async_computation.6 | async-start | bytes 147456 | tf_op jit(solution)/shard_map/reduce_scatter | solution.py:105
  31.1 12.5 %copy-start.11 = (f32[16,2]{0,1:T(2,128)}, f32[16,2]{0,1:T(2,128)S(1)}, u32[]{:S(2)}) copy-start(f32[16,2]{0,1:T(2,128)S(1)} %fusion.58) | copy-start | bytes 388
  37.5 8.3 %copy-start.9 = (s32[16,1]{0,1:T(1,128)S(1)}, s32[16,1]{0,1:T(1,128)}, u32[]{:S(2)}) copy-start(s32[16,1]{0,1:T(1,128)} %param.36) | copy-start | bytes 196
  37.5 8.6 %copy-start.12 = (f32[16,2]{0,1:T(2,128)S(1)}, f32[16,2]{0,1:T(2,128)}, u32[]{:S(2)}) copy-start(f32[16,2]{0,1:T(2,128)} %param.39) | copy-start | bytes 388
  37.6 8.6 %copy-start.14 = (f32[16]{0:T(128)S(1)}, f32[16]{0:T(128)}, u32[]{:S(2)}) copy-start(f32[16]{0:T(128)} %param.38) | copy-start | bytes 196
  37.6 8.6 %copy-start.10 = (s32[16,2]{0,1:T(2,128)S(1)}, s32[16,2]{0,1:T(2,128)}, u32[]{:S(2)}) copy-start(s32[16,2]{0,1:T(2,128)} %param.37) | copy-start | bytes 388
  37.6 40.0 %copy-start.8 = (bf16[16,256]{1,0:T(8,128)(2,1)S(1)}, bf16[16,256]{1,0:T(8,128)(2,1)}, u32[]{:S(2)}) copy-start(bf16[16,256]{1,0:T(8,128)(2,1)} %param.23) | copy-start | bytes 24580
  37.6 54.8 %copy-start.6 = (f32[2048]{0:T(1024)S(1)}, f32[2048]{0:T(1024)}, u32[]{:S(2)}) copy-start(f32[2048]{0:T(1024)} %param.35) | copy-start | bytes 24580
  38.8 67.3 %copy-start.7 = (bf16[16,2,128]{2,1,0:T(2,128)(2,1)}, bf16[16,2,128]{2,1,0:T(2,128)(2,1)S(1)}, u32[]{:S(2)}) copy-start(bf16[16,2,128]{2,1,0:T(2,128)(2,1)S(1)} %convert_element_type.102) | copy-start | bytes 24580
  38.8 67.3 %copy-start.1 = (bf16[256,2048]{1,0:T(8,128)(2,1)S(1)}, bf16[256,2048]{1,0:T(8,128)(2,1)}, u32[]{:S(2)}) copy-start(bf16[256,2048]{1,0:T(8,128)(2,1)} %param.44) | copy-start | bytes 3145732
  38.8 67.3 %copy-start.2 = (bf16[2048,256]{1,0:T(8,128)(2,1)S(1)}, bf16[2048,256]{1,0:T(8,128)(2,1)}, u32[]{:S(2)}) copy-start(bf16[2048,256]{1,0:T(8,128)(2,1)} %param.43) | copy-start | bytes 3145732
  38.9 99.9 %copy-start.13 = (f32[256]{0:T(256)S(1)}, f32[256]{0:T(256)}, u32[]{:S(2)}) copy-start(f32[256]{0:T(256)} %param.45) | copy-start | bytes 3076
  47.0 46.2 %all-to-all-start.1 = ((bf16[4,8,4]{1,2,0:T(4,128)(2,1)}), bf16[4,8,4]{1,2,0:T(4,128)(2,1)S(1)}, u32[]{:S(2)}, u32[]{:S(2)}) async-start(bf16[4,8,4]{1,2,0:T(4,128)(2,1)} %copy.49), calls=%async_computation.2 | async-start | bytes 8192 | tf_op jit(solution)/shard_map/all_to_all | solution.py:128
  93.2 8.7 %all-to-all-start = ((bf16[4,8,2048]{2,1,0:T(8,128)(2,1)}), bf16[4,8,2048]{2,1,0:T(8,128)(2,1)S(1)}, u32[]{:S(2)}, u32[]{:S(2)}) async-start(bf16[4,8,2048]{2,1,0:T(8,128)(2,1)} %fusion), calls=%async_computation.1 | async-start | bytes 262144 | tf_op jit(solution)/shard_map/all_to_all | solution.py:127
  96.9 36.9 %reduce-scatter.6.cloned.1.call-start = ((), (), s32[]{:S(2)}) async-start(), calls=%async_computation.7 | async-start | bytes 294912 | tf_op jit(solution)/shard_map/reduce_scatter | solution.py:145
  106.1 58.6 %reduce-scatter.8.cloned.1.call-start = ((), (), s32[]{:S(2)}) async-start(), calls=%async_computation.8 | async-start | bytes 147456 | tf_op jit(solution)/shard_map/reduce_scatter | solution.py:146
  135.1 29.6 %all-to-all-start.2 = ((bf16[4,8,256]{2,1,0:T(8,128)(2,1)}), bf16[4,8,256]{2,1,0:T(8,128)(2,1)S(1)}, u32[]{:S(2)}, u32[]{:S(2)}) async-start(bf16[4,8,256]{2,1,0:T(8,128)(2,1)} %convert_bitcast_fusion), calls=%async_computation.4 | async-start | bytes 32768 | tf_op jit(solution)/shard_map/all_to_all | solution.py:148
Sparse Core Ops, SparseCore 0:
  45.9 31.5 reduce-scatter.3
  106.2 27.4 reduce-scatter.5
  136.0 28.7 reduce-scatter.7
where the time goes:
time: 174 us; the launch traced here: 173 us
  waiting for transfers between devices  83.8 us (48%)
  blocking collectives  29.8 us (17%)
  matrix products  24.9 us (14%)
  between operations  14 us (8%)
  starting transfers between devices  11 us (6%)
  other arithmetic  7.35 us (4%)
  local copies, waits for them, and re-layouts  1.82 us (1%)
    reduce_scatter x1, waiting for transfers between devices, body(): lax.psum_scatter(partial_value, 'tp', scatter_dimension=1, tiled=True)  26.8 us
    reduce_scatter x1, waiting for transfers between devices, body(): lax.psum_scatter(expert_part, 'tp', scatter_dimension=1, tiled=True)  26.1 us
    reduce_scatter x1, waiting for transfers between devices, body(): lax.psum_scatter(dense_part, 'tp', scatter_dimension=1, tiled=True)  26 us
    all_gather x1, blocking collectives, body(): gathered = lax.all_gather(tokens, 'tp', axis=1, tiled=True)  15.9 us
    all_gather x1, blocking collectives, body(): lax.all_gather(own_residual, 'tp', axis=1, tiled=True)  13.9 us
    dot_general x1, matrix products, attend(): jnp.einsum('shd,shld->shl', queries, key_cache, preferred_element_type=jn...  5.63 us
    all_to_all x1, waiting for transfers between devices, body(): lax.all_to_all(send_rows, 'ep', split_axis=0, concat_axis=0, tiled=True)  4.85 us
    dot_general x1, matrix products, attend(): jnp.einsum('shl,shld->shd', weights, value_cache, preferred_element_type=...  4.72 us
  transfers between devices with their start and end apart: 6, of which 4 were waited for; matrix products, arithmetic and copies ran while one was open for 3% of the time, Pallas kernels for 0%

commit v1 on v0

--- a/solution.py
+++ b/solution.py
@@ -7,6 +7,23 @@
 EPG = 4
 EPS = 1e-06
 FLOOR = -1e30
+
+
+def laid_out(tiles, dim):
+    tiles = jnp.moveaxis(tiles, 0, dim)
+    dims = tiles.shape
+    return tiles.reshape(*dims[:dim], dims[dim] * dims[dim + 1], *dims[dim + 2 :])
+
+
+def collect(shard, axis, dim):
+    size = lax.axis_size(axis)
+    ahead = [(i, (i + 1) % size) for i in range(size)]
+    tiles = [shard]
+    while len(tiles) < size:
+        tiles.append(lax.ppermute(tiles[-1], axis, ahead))
+    mine = lax.axis_index(axis)
+    tiles = jnp.stack(tiles)[(mine - jnp.arange(size)) % size]
+    return laid_out(tiles, dim)
 
 
 def norm_rows(row_data, gain_vec):
@@ -104,7 +121,7 @@
     )
     piece_sum = lax.psum_scatter(partial_value, "tp", scatter_dimension=1, tiled=True)
     own_residual = (tokens.astype(jnp.float32) + piece_sum).astype(jnp.bfloat16)
-    moe_in = norm_rows(lax.all_gather(own_residual, "tp", axis=1, tiled=True), moe_gain)
+    moe_in = norm_rows(collect(own_residual, "tp", 1), moe_gain)
     groups = lax.axis_size("ep")
     capacity = max(2, 2 * seq_count // groups)
     first_share = jax.nn.sigmoid(pair_logits[:, 0] - pair_logits[:, 1])

time: 174 us -> 192 us (1.10)
  waiting for transfers between devices: 83.8 us -> 116 us
  blocking collectives: 29.8 us -> 15.9 us
    ppermute x0 -> x7, waiting for transfers between devices: none -> 34.1 us  [collect(): tiles.append(lax.ppermute(tiles[-1], axis, ahead))]
    all_gather x1 -> x0, blocking collectives: 13.9 us -> none  [body(): lax.all_gather(own_residual, 'tp', axis=1, tiled=True)]
  transfers between devices with their start and end apart: 6 -> 13, of which waited for: 4 -> 11; matrix products, arithmetic and copies ran while one was open for 3% -> 4% of each run, Pallas kernels for 0% -> 0%
where the time goes in v1:
time: 192 us; the launch traced here: 191 us
  waiting for transfers between devices  116 us (60%)
  matrix products  23.9 us (12%)
  blocking collectives  15.9 us (8%)
  between operations  14.1 us (7%)
  starting transfers between devices  11 us (6%)
  other arithmetic  7.33 us (4%)
  local copies, waits for them, and re-layouts  2.38 us (1%)
    ppermute x7, waiting for transfers between devices, collect(): tiles.append(lax.ppermute(tiles[-1], axis, ahead))  34.1 us
    reduce_scatter x1, waiting for transfers between devices, body(): lax.psum_scatter(partial_value, 'tp', scatter_dimension=1, tiled=True)  26.8 us
    reduce_scatter x1, waiting for transfers between devices, body(): lax.psum_scatter(dense_part, 'tp', scatter_dimension=1, tiled=True)  25.9 us
    reduce_scatter x1, waiting for transfers between devices, body(): lax.psum_scatter(expert_part, 'tp', scatter_dimension=1, tiled=True)  24.6 us
    all_gather x1, blocking collectives, body(): gathered = lax.all_gather(tokens, 'tp', axis=1, tiled=True)  15.9 us
    dot_general x1, matrix products, attend(): jnp.einsum('shd,shld->shl', queries, key_cache, preferred_element_type=jn...  5.63 us
    all_to_all x1, waiting for transfers between devices, body(): lax.all_to_all(send_rows, 'ep', split_axis=0, concat_axis=0, tiled=True)  4.85 us
    dot_general x1, matrix products, attend(): jnp.einsum('shl,shld->shd', weights, value_cache, preferred_element_type=...  4.58 us
  transfers between devices with their start and end apart: 13, of which 11 were waited for; matrix products, arithmetic and copies ran while one was open for 4% of the time, Pallas kernels for 0%

profile of v1, /device:TPU:0, one launch (start us, length us, event | category | flops | bytes accessed | tf_op | source)
XLA Modules:
  0.0 190.8 jit_solution(7869532155157101747)
XLA Ops:
  8.7 15.9 %all_gather.3 = bf16[16,2048]{1,0:T(8,128)(2,1)S(1)} all-gather(bf16[16,256]{1,0:T(8,128)(2,1)} %param.23), channel_id=1, replica_groups=mesh['ep'=4,'tp'=8] {'tp'}, dimensions={1}, use_global_device_ids=true | all-gather | bytes 73728 | tf_op jit(solution)/shard_map/all_gather | solution.py:91
  24.8 1.5 fusion.61
  26.4 1.5 fusion.64
  28.1 1.1 select_reduce_fusion
  31.8 5.6 %fusion.32 = f32[16,2,1,1024]{3,2,1,0:T(1,128)S(1)} fusion(bf16[16,2,1024,128]{3,2,1,0:T(8,128)(2,1)} %param.24, bf16[16,2,128,1]{2,1,0,3:T(2,128)(2,1)S(1)} %get-tuple-element.14), kind=kOutput, calls=%fused_computation.56 | convolution fusion | flops 8388608 | bytes 8527872 | tf_op jit(solution)/shard_map/shd,shld->shl/dot_general | solution.py:43
  38.8 4.6 %fusion.22 = f32[16,2,1,128]{3,2,1,0:T(1,128)S(1)} fusion(bf16[16,2,1024,128]{3,2,1,0:T(8,128)(2,1)} %param.25, bf16[16,2,1024,1]{2,1,0,3:T(2,128)(2,1)S(1)} %fusion.24), kind=kOutput, calls=%fused_computation.32 | convolution fusion | flops 8388608 | bytes 8470528 | tf_op jit(solution)/shard_map/shl,shld->shd/dot_general | solution.py:59
  45.6 3.7 %all-to-all-start.1 = ((bf16[4,8,4]{1,2,0:T(4,128)(2,1)}), bf16[4,8,4]{1,2,0:T(4,128)(2,1)S(1)}, u32[]{:S(2)}, u32[]{:S(2)}) async-start(bf16[4,8,4]{1,2,0:T(4,128)(2,1)} %copy.57), calls=%async_computation.2 | async-start | bytes 8192 | tf_op jit(solution)/shard_map/all_to_all | solution.py:145
  49.4 26.8 %reduce-scatter.4.cloned.1.call-done = f32[16,256]{1,0:T(8,128)} async-done(((f32[16,2048]{1,0:T(8,128)}), f32[16,256]{1,0:T(8,128)}) %reduce-scatter.4.cloned.1.call-update) | async-done | bytes 16400 | tf_op jit(solution)/shard_map/reduce_scatter | solution.py:122
  76.9 4.9 %collective-permute-done = bf16[16,256]{1,0:T(8,128)(2,1)S(1)} collective-permute-done((bf16[16,256]{1,0:T(8,128)(2,1)S(1)}, bf16[16,256]{1,0:T(8,128)(2,1)S(1)}, u32[]{:S(2)}, u32[]{:S(2)}) %collective-permute-start) | collective-permute-done | bytes 8224 | tf_op jit(solution)/shard_map/ppermute | solution.py:23
  81.7 4.9 %collective-permute-done.1 = bf16[16,256]{1,0:T(8,128)(2,1)S(1)} collective-permute-done((bf16[16,256]{1,0:T(8,128)(2,1)S(1)}, bf16[16,256]{1,0:T(8,128)(2,1)S(1)}, u32[]{:S(2)}, u32[]{:S(2)}) %collective-permute-start.1) | collective-permute-done | bytes 8224 | tf_op jit(solution)/shard_map/ppermute | solution.py:23
  86.6 4.9 %collective-permute-done.2 = bf16[16,256]{1,0:T(8,128)(2,1)S(1)} collective-permute-done((bf16[16,256]{1,0:T(8,128)(2,1)S(1)}, bf16[16,256]{1,0:T(8,128)(2,1)S(1)}, u32[]{:S(2)}, u32[]{:S(2)}) %collective-permute-start.2) | collective-permute-done | bytes 8224 | tf_op jit(solution)/shard_map/ppermute | solution.py:23
  91.5 4.9 %collective-permute-done.3 = bf16[16,256]{1,0:T(8,128)(2,1)S(1)} collective-permute-done((bf16[16,256]{1,0:T(8,128)(2,1)S(1)}, bf16[16,256]{1,0:T(8,128)(2,1)S(1)}, u32[]{:S(2)}, u32[]{:S(2)}) %collective-permute-start.3) | collective-permute-done | bytes 8224 | tf_op jit(solution)/shard_map/ppermute | solution.py:23
  96.4 4.9 %collective-permute-done.4 = bf16[16,256]{1,0:T(8,128)(2,1)S(1)} collective-permute-done((bf16[16,256]{1,0:T(8,128)(2,1)S(1)}, bf16[16,256]{1,0:T(8,128)(2,1)S(1)}, u32[]{:S(2)}, u32[]{:S(2)}) %collective-permute-start.4) | collective-permute-done | bytes 8224 | tf_op jit(solution)/shard_map/ppermute | solution.py:23
  101.2 4.9 %collective-permute-done.5 = bf16[16,256]{1,0:T(8,128)(2,1)S(1)} collective-permute-done((bf16[16,256]{1,0:T(8,128)(2,1)S(1)}, bf16[16,256]{1,0:T(8,128)(2,1)S(1)}, u32[]{:S(2)}, u32[]{:S(2)}) %collective-permute-start.5) | collective-permute-done | bytes 8224 | tf_op jit(solution)/shard_map/ppermute | solution.py:23
  106.1 4.9 %collective-permute-done.6 = bf16[16,256]{1,0:T(8,128)(2,1)S(1)} collective-permute-done((bf16[16,256]{1,0:T(8,128)(2,1)S(1)}, bf16[16,256]{1,0:T(8,128)(2,1)S(1)}, u32[]{:S(2)}, u32[]{:S(2)}) %collective-permute-start.6) | collective-permute-done | bytes 8224 | tf_op jit(solution)/shard_map/ppermute | solution.py:23
  112.6 3.6 %all-to-all-start = ((bf16[4,8,2048]{2,1,0:T(8,128)(2,1)}), bf16[4,8,2048]{2,1,0:T(8,128)(2,1)S(1)}, u32[]{:S(2)}, u32[]{:S(2)}) async-start(bf16[4,8,2048]{2,1,0:T(8,128)(2,1)} %fusion), calls=%async_computation.1 | async-start | bytes 262144 | tf_op jit(solution)/shard_map/all_to_all | solution.py:144
  116.4 4.8 %all-to-all-done = bf16[4,8,2048]{2,1,0:T(8,128)(2,1)S(1)} async-done(((bf16[4,8,2048]{2,1,0:T(8,128)(2,1)}), bf16[4,8,2048]{2,1,0:T(8,128)(2,1)S(1)}, u32[]{:S(2)}, u32[]{:S(2)}) %all-to-all-start) | async-done | bytes 131104 | tf_op jit(solution)/shard_map/all_to_all | solution.py:144
  121.6 2.7 %fusion.4 = f32[32,2048]{1,0:T(8,128)} fusion(bf16[1,256,2048]{2,1,0:T(8,128)(2,1)S(1)} %copy-done, bf16[1,2048,256]{2,1,0:T(8,128)(2,1)} %param.41, bf16[4,8,2048]{2,1,0:T(8,128)(2,1)S(1)} %all-to-all-done, f32[32,256]{1,0:T(8,128)S(1)} %fusion.10, f32[32]{0:T(128)S(1)} %mul.183), kind=kOutput, calls=%fused_computation.8 | convolution fusion | flops 67166208 | bytes 2523264 | tf_op jit(solution)/shard_map/dot_general | solution.py:160
  124.3 3.0 %fusion.36 = f32[16,2048]{1,0:T(8,128)} fusion(bf16[256,2048]{1,0:T(8,128)(2,1)} %param.44, bf16[2048,256]{1,0:T(8,128)(2,1)} %param.43, f32[16,2048]{1,0:T(8,128)S(1)} %bitcast.78, f32[2048]{0:T(1024)S(1)} %copy-done.8, f32[16]{0:T(128)S(1)} %add_rsqrt_fusion.2), kind=kOutput, calls=%fused_computation.70 | convolution fusion | flops 33673216 | bytes 2367552 | tf_op jit(solution)/shard_map/dot_general | solution.py:150
  127.3 24.6 %reduce-scatter.6.cloned.1.call-done = f32[32,256]{1,0:T(8,128)} async-done(((f32[32,2048]{1,0:T(8,128)}), f32[32,256]{1,0:T(8,128)}) %reduce-scatter.6.cloned.1.call-update) | async-done | bytes 32784 | tf_op jit(solution)/shard_map/reduce_scatter | solution.py:162
  151.9 1.4 convert_bitcast_fusion.1
  153.3 3.6 %all-to-all-start.2 = ((bf16[4,8,256]{2,1,0:T(8,128)(2,1)}), bf16[4,8,256]{2,1,0:T(8,128)(2,1)S(1)}, u32[]{:S(2)}, u32[]{:S(2)}) async-start(bf16[4,8,256]{2,1,0:T(8,128)(2,1)} %convert_bitcast_fusion.1), calls=%async_computation.4 | async-start | bytes 32768 | tf_op jit(solution)/shard_map/all_to_all | solution.py:165
  156.8 25.9 %reduce-scatter.8.cloned.1.call-done = f32[16,256]{1,0:T(8,128)} async-done(((f32[16,2048]{1,0:T(8,128)}), f32[16,256]{1,0:T(8,128)}) %reduce-scatter.8.cloned.1.call-update) | async-done | bytes 16400 | tf_op jit(solution)/shard_map/reduce_scatter | solution.py:163
  182.8 1.5 fusion.5
  (100 shorter events, 10.9 us)
Async XLA Ops:
  7.2 114.4 %copy-start = (bf16[1,256,2048]{2,1,0:T(8,128)(2,1)S(1)}, bf16[1,256,2048]{2,1,0:T(8,128)(2,1)}, u32[]{:S(2)}) copy-start(bf16[1,256,2048]{2,1,0:T(8,128)(2,1)} %param.42) | copy-start | bytes 3145732
  7.2 31.3 %copy-start.5 = (f32[2048]{0:T(1024)S(1)}, f32[2048]{0:T(1024)}, u32[]{:S(2)}) copy-start(f32[2048]{0:T(1024)} %param.28) | copy-start | bytes 24580
  7.2 30.3 %copy-start.4 = (f32[16,2,1024]{2,1,0:T(2,128)S(1)}, f32[16,2,1024]{2,1,0:T(2,128)}, u32[]{:S(2)}) copy-start(f32[16,2,1024]{2,1,0:T(2,128)} %param.26) | copy-start | bytes 393220
  7.2 68.9 %reduce-scatter.4.cloned.1.call-start = ((), (), s32[]{:S(2)}) async-start(), calls=%async_computation.6 | async-start | bytes 147456 | tf_op jit(solution)/shard_map/reduce_scatter | solution.py:122
  31.0 12.3 %copy-start.11 = (f32[16,2]{0,1:T(2,128)}, f32[16,2]{0,1:T(2,128)S(1)}, u32[]{:S(2)}) copy-start(f32[16,2]{0,1:T(2,128)S(1)} %fusion.49) | copy-start | bytes 388
  31.1 7.3 %copy-start.3 = (bf16[2048,256]{1,0:T(8,128)(2,1)S(1)}, bf16[2048,256]{1,0:T(8,128)(2,1)}, u32[]{:S(2)}) copy-start(bf16[2048,256]{1,0:T(8,128)(2,1)} %param.31) | copy-start | bytes 3145732
  37.5 7.2 %copy-start.10 = (s32[16,2]{0,1:T(2,128)S(1)}, s32[16,2]{0,1:T(2,128)}, u32[]{:S(2)}) copy-start(s32[16,2]{0,1:T(2,128)} %param.37) | copy-start | bytes 388
  37.5 38.6 %copy-start.6 = (bf16[16,256]{1,0:T(8,128)(2,1)S(1)}, bf16[16,256]{1,0:T(8,128)(2,1)}, u32[]{:S(2)}) copy-start(bf16[16,256]{1,0:T(8,128)(2,1)} %param.23) | copy-start | bytes 24580
  37.9 73.9 %copy-start.8 = (f32[2048]{0:T(1024)S(1)}, f32[2048]{0:T(1024)}, u32[]{:S(2)}) copy-start(f32[2048]{0:T(1024)} %param.35) | copy-start | bytes 24580
  38.5 82.8 %copy-start.2 = (bf16[1,2048,256]{2,1,0:T(8,128)(2,1)S(1)}, bf16[1,2048,256]{2,1,0:T(8,128)(2,1)}, u32[]{:S(2)}) copy-start(bf16[1,2048,256]{2,1,0:T(8,128)(2,1)} %param.40) | copy-start | bytes 3145732
  38.8 82.8 %copy-start.7 = (bf16[16,2,128]{2,1,0:T(2,128)(2,1)}, bf16[16,2,128]{2,1,0:T(2,128)(2,1)S(1)}, u32[]{:S(2)}) copy-start(bf16[16,2,128]{2,1,0:T(2,128)(2,1)S(1)} %convert_element_type.112) | copy-start | bytes 24580
  38.8 118.0 %copy-start.13 = (f32[256]{0:T(256)S(1)}, f32[256]{0:T(256)}, u32[]{:S(2)}) copy-start(f32[256]{0:T(256)} %param.45) | copy-start | bytes 3076
  45.6 67.0 %all-to-all-start.1 = ((bf16[4,8,4]{1,2,0:T(4,128)(2,1)}), bf16[4,8,4]{1,2,0:T(4,128)(2,1)S(1)}, u32[]{:S(2)}, u32[]{:S(2)}) async-start(bf16[4,8,4]{1,2,0:T(4,128)(2,1)} %copy.57), calls=%async_computation.2 | async-start | bytes 8192 | tf_op jit(solution)/shard_map/all_to_all | solution.py:145
  76.9 4.9 %collective-permute-start = (bf16[16,256]{1,0:T(8,128)(2,1)S(1)}, bf16[16,256]{1,0:T(8,128)(2,1)S(1)}, u32[]{:S(2)}, u32[]{:S(2)}) collective-permute-start(bf16[16,256]{1,0:T(8,128)(2,1)S(1)} %get-tuple-element.7), channel_id=1, source_target_pairs={{0,1},{1,2},{2,3},{3,4},{4,5},{5,6},{6,7},{7,0},{8,9},{9,10},{10,1... | collective-permute-start | bytes 24584 | tf_op jit(solution)/shard_map/ppermute | solution.py:23
  81.7 4.9 %collective-permute-start.1 = (bf16[16,256]{1,0:T(8,128)(2,1)S(1)}, bf16[16,256]{1,0:T(8,128)(2,1)S(1)}, u32[]{:S(2)}, u32[]{:S(2)}) collective-permute-start(bf16[16,256]{1,0:T(8,128)(2,1)S(1)} %collective-permute-done), channel_id=1, source_target_pairs={{0,1},{1,2},{2,3},{3,4},{4,5},{5,6},{6,7},{7,0},{8,9},{9,10},{10,1... | collective-permute-start | bytes 24584 | tf_op jit(solution)/shard_map/ppermute | solution.py:23
  86.6 4.9 %collective-permute-start.2 = (bf16[16,256]{1,0:T(8,128)(2,1)S(1)}, bf16[16,256]{1,0:T(8,128)(2,1)S(1)}, u32[]{:S(2)}, u32[]{:S(2)}) collective-permute-start(bf16[16,256]{1,0:T(8,128)(2,1)S(1)} %collective-permute-done.1), channel_id=1, source_target_pairs={{0,1},{1,2},{2,3},{3,4},{4,5},{5,6},{6,7},{7,0},{8,9},{9,10},{10,1... | collective-permute-start | bytes 24584 | tf_op jit(solution)/shard_map/ppermute | solution.py:23
  91.5 4.9 %collective-permute-start.3 = (bf16[16,256]{1,0:T(8,128)(2,1)S(1)}, bf16[16,256]{1,0:T(8,128)(2,1)S(1)}, u32[]{:S(2)}, u32[]{:S(2)}) collective-permute-start(bf16[16,256]{1,0:T(8,128)(2,1)S(1)} %collective-permute-done.2), channel_id=1, source_target_pairs={{0,1},{1,2},{2,3},{3,4},{4,5},{5,6},{6,7},{7,0},{8,9},{9,10},{10,1... | collective-permute-start | bytes 24584 | tf_op jit(solution)/shard_map/ppermute | solution.py:23
  96.4 4.9 %collective-permute-start.4 = (bf16[16,256]{1,0:T(8,128)(2,1)S(1)}, bf16[16,256]{1,0:T(8,128)(2,1)S(1)}, u32[]{:S(2)}, u32[]{:S(2)}) collective-permute-start(bf16[16,256]{1,0:T(8,128)(2,1)S(1)} %collective-permute-done.3), channel_id=1, source_target_pairs={{0,1},{1,2},{2,3},{3,4},{4,5},{5,6},{6,7},{7,0},{8,9},{9,10},{10,1... | collective-permute-start | bytes 24584 | tf_op jit(solution)/shard_map/ppermute | solution.py:23
  101.2 4.9 %collective-permute-start.5 = (bf16[16,256]{1,0:T(8,128)(2,1)S(1)}, bf16[16,256]{1,0:T(8,128)(2,1)S(1)}, u32[]{:S(2)}, u32[]{:S(2)}) collective-permute-start(bf16[16,256]{1,0:T(8,128)(2,1)S(1)} %collective-permute-done.4), channel_id=1, source_target_pairs={{0,1},{1,2},{2,3},{3,4},{4,5},{5,6},{6,7},{7,0},{8,9},{9,10},{10,1... | collective-permute-start | bytes 24584 | tf_op jit(solution)/shard_map/ppermute | solution.py:23
  106.1 4.9 %collective-permute-start.6 = (bf16[16,256]{1,0:T(8,128)(2,1)S(1)}, bf16[16,256]{1,0:T(8,128)(2,1)S(1)}, u32[]{:S(2)}, u32[]{:S(2)}) collective-permute-start(bf16[16,256]{1,0:T(8,128)(2,1)S(1)} %collective-permute-done.5), channel_id=1, source_target_pairs={{0,1},{1,2},{2,3},{3,4},{4,5},{5,6},{6,7},{7,0},{8,9},{9,10},{10,1... | collective-permute-start | bytes 24584 | tf_op jit(solution)/shard_map/ppermute | solution.py:23
  112.6 8.7 %all-to-all-start = ((bf16[4,8,2048]{2,1,0:T(8,128)(2,1)}), bf16[4,8,2048]{2,1,0:T(8,128)(2,1)S(1)}, u32[]{:S(2)}, u32[]{:S(2)}) async-start(bf16[4,8,2048]{2,1,0:T(8,128)(2,1)} %fusion), calls=%async_computation.1 | async-start | bytes 262144 | tf_op jit(solution)/shard_map/all_to_all | solution.py:144
  116.2 35.7 %reduce-scatter.6.cloned.1.call-start = ((), (), s32[]{:S(2)}) async-start(), calls=%async_computation.7 | async-start | bytes 294912 | tf_op jit(solution)/shard_map/reduce_scatter | solution.py:162
  124.3 58.5 %reduce-scatter.8.cloned.1.call-start = ((), (), s32[]{:S(2)}) async-start(), calls=%async_computation.8 | async-start | bytes 147456 | tf_op jit(solution)/shard_map/reduce_scatter | solution.py:163
  153.3 29.5 %all-to-all-start.2 = ((bf16[4,8,256]{2,1,0:T(8,128)(2,1)}), bf16[4,8,256]{2,1,0:T(8,128)(2,1)S(1)}, u32[]{:S(2)}, u32[]{:S(2)}) async-start(bf16[4,8,256]{2,1,0:T(8,128)(2,1)} %convert_bitcast_fusion.1), calls=%async_computation.4 | async-start | bytes 32768 | tf_op jit(solution)/shard_map/all_to_all | solution.py:165
  (4 other events, 27.4 us)
Sparse Core Ops, SparseCore 0:
  44.5 31.5 reduce-scatter.3
  124.4 27.4 reduce-scatter.5
  154.2 28.5 reduce-scatter.7
